TPU v7x, 512 devices: a 4x2x32 block of a 4x8x32 slice. The times are simulated.
512 devices in a mesh: grp: 2 (over y), ra: 32 (over z), cb: 8 (over x, core).
Axes of the slice: x: 4, y: 2, z: 32, core: 2. Of those that a mesh axis runs over, the one named last changes fastest.
The devices are a block of a 4x8x32 slice.
Arguments:
- stream: bfloat16 [256, 4096], P('grp', 'ra'), parts along dimension 0, may hold values from -180 to 180
- w_gate: float32 [2, 4096, 11264], P(None, 'ra', 'cb'), may hold values from -0.09375 to 0.09375
- w_up: float32 [2, 4096, 11264], P(None, 'ra', 'cb'), may hold values from -0.09375 to 0.09375
- w_down: float32 [2, 11264, 4096], P(None, 'cb', 'ra'), may hold values from -0.0546875 to 0.0546875
- gate_scale: float32 [2, 11264], P(None, 'cb'), may hold values from 0.5 to 2
- up_scale: float32 [2, 11264], P(None, 'cb'), may hold values from 0.5 to 2
- down_scale: float32 [2, 4096], P(None, 'ra'), may hold values from 0.5 to 2
- pre_gain: float32 [2, 4096], P(None, 'ra'), may hold values from 0.1 to 1.9
- out_gain: float32 [4096], P('ra'), may hold values from 0.1 to 1.9
Outputs:
- normed: bfloat16 [256, 4096], P('grp', 'ra'), parts along dimension 0
There are 2 independent parts, one for each index of `grp`. A program takes and returns all parts, laid end to end along the dimension named above; an argument that names none is the same for every part. Nothing has to cross between parts.
All inputs are finite; a program needn't handle non-finite values.
Results may differ from a plain program's by a relative error of at most 0.018.
Values may be sent and summed in bfloat16 or wider, within the bound.
A program may use at most 64 MiB of HBM per device.

v0:
```python
import jax
import jax.numpy as jnp
from jax import lax
from jax.sharding import PartitionSpec as P

D = 4096
LAYERS = 2


def cut_along(shard, dim, size):
    before, after = (shard.shape[:dim], shard.shape[dim + 1 :])
    return jnp.moveaxis(shard.reshape(*before, size, -1, *after), dim, 0)


def one_scatter(arrays, axis, dims):
    size = lax.axis_size(axis)
    tiles = [cut_along(a, dim, size) for a, dim in zip(arrays, dims)]
    lines = jnp.concatenate([b.reshape(size, -1) for b in tiles], axis=1)
    width = max(16, -(-lines.shape[1] // 1024) * 8)
    lines = jnp.pad(lines, ((0, 0), (0, width * 128 - lines.shape[1]))).reshape(-1, 128)
    line, at, finished = (lax.psum_scatter(lines, axis, tiled=True).reshape(-1), 0, [])
    for b in tiles:
        part = b[0]
        finished.append(line[at : at + part.size].reshape(part.shape))
        at += part.size
    return tuple(finished)


def sent_to_all(shard, axis):
    copies = jnp.broadcast_to(shard, (lax.axis_size(axis), *shard.shape))
    return lax.all_to_all(copies, axis, split_axis=0, concat_axis=0, tiled=True)


def laid_out(tiles, dim):
    tiles = jnp.moveaxis(tiles, 0, dim)
    lengths = tiles.shape
    return tiles.reshape(*lengths[:dim], lengths[dim] * lengths[dim + 1], *lengths[dim + 2 :])


def collect(shard, axis, dim):
    tiles = sent_to_all(shard, axis)
    return laid_out(tiles, dim)


def taken_together(shard, axis):
    return sent_to_all(shard, axis).astype(jnp.float32).sum(axis=0)


def over_copies(shard, axis):
    return sent_to_all(shard, axis).sum(axis=0)


def local(stream, w_gate, w_up, w_down, gate_scale, up_scale, down_scale, pre_gain, out_gain):
    current = stream
    for layer in range(LAYERS):
        xvals = current.astype(jnp.float32)
        squares = jnp.sum(xvals * xvals, axis=1)
        scaled = (xvals * pre_gain[layer]).astype(jnp.bfloat16)
        gate_part = jnp.dot(
            scaled, w_gate[layer].astype(jnp.bfloat16), preferred_element_type=jnp.float32
        )
        up_part = jnp.dot(
            scaled, w_up[layer].astype(jnp.bfloat16), preferred_element_type=jnp.float32
        )
        down_local = w_down[layer].astype(jnp.bfloat16)
        operands = (gate_part, up_part, squares)
        summed = one_scatter((operands[0], operands[1], operands[2]), "ra", (0, 0, 0))
        own_rows = summed[2]
        rinv = lax.rsqrt(own_rows / D + 1e-06)[:, None]
        gate = summed[0] * rinv * gate_scale[layer]
        upper = summed[1] * rinv * up_scale[layer]
        hidden = (jax.nn.silu(gate) * upper).astype(jnp.bfloat16)
        terms = jnp.dot(collect(hidden, "ra", 0), down_local, preferred_element_type=jnp.float32)
        branch = (
            taken_together(terms.astype(jnp.bfloat16), "cb").astype(jnp.float32) * down_scale[layer]
        )
        current = (0.5 * xvals + branch).astype(jnp.bfloat16)
    xvals = current.astype(jnp.float32)
    final_sum = over_copies(jnp.sum(xvals * xvals, axis=1), "ra")
    rinv = lax.rsqrt(final_sum / D + 1e-06)[:, None]
    return (xvals * rinv * out_gain).astype(jnp.bfloat16)


def solution(mesh):
    placed = (
        P("grp", "ra"),
        P(None, "ra", "cb"),
        P(None, "ra", "cb"),
        P(None, "cb", "ra"),
        P(None, "cb"),
        P(None, "cb"),
        P(None, "ra"),
        P(None, "ra"),
        P("ra"),
    )
    return jax.shard_map(
        local, mesh=mesh, in_specs=placed, out_specs=P("grp", "ra"), check_vma=False
    )
```

profile of v0, /device:TPU:33, one launch (start us, length us, event | category | flops | bytes accessed | tf_op | source)
XLA Modules:
  0.0 464.7 jit_solution(1497462713753054547)
XLA Ops:
  6.6 0.8 slice_bitcast_fusion.13
  7.3 1.4 convert.12
  8.8 0.1 fusion.10
  8.9 0.3 fusion.3
  9.1 1.0 reshape_reshape.12
  10.1 0.1 convert.13
  10.2 0.2 fusion.2
  10.5 1.0 reshape_reshape.13
  11.4 0.1 reshape.62
  11.5 1.4 select_maximum_fusion.2
  13.0 1.4 reshape.63
  14.4 0.1 reduce-scatter.3.cloned.1.call-update
  14.4 0.6 copy-done.4
  15.1 0.1 slice_reduce_fusion
  15.1 138.7 %reduce-scatter.3.cloned.1.call-done = f32[96,128]{1,0:T(8,128)} async-done(((f32[3072,128]{1,0:T(8,128)}), f32[96,128]{1,0:T(8,128)}) %reduce-scatter.3.cloned.1.call-update) | async-done | bytes 49168 | tf_op jit(solution)/shard_map/reduce_scatter | solution.py:21
  153.8 0.8 fusion.30
  154.7 0.7 fusion.26
  155.4 0.1 fusion.22
  155.5 0.8 broadcast_in_dim.19
  156.3 15.9 %all-to-all-start = ((bf16[32,4,1408]{2,1,0:T(4,128)(2,1)}), bf16[32,4,1408]{2,1,0:T(4,128)(2,1)S(1)}, u32[]{:S(2)}, u32[]{:S(2)}) async-start(bf16[32,4,1408]{2,1,0:T(4,128)(2,1)} %broadcast_in_dim.19), calls=%async_computation.1 | async-start | bytes 720896 | tf_op jit(solution)/shard_map/all_to_all | solution.py:31
  172.2 1.0 convert.14
  173.2 34.3 %all-to-all-done = bf16[32,4,1408]{2,1,0:T(4,128)(2,1)S(1)} async-done(((bf16[32,4,1408]{2,1,0:T(4,128)(2,1)}), bf16[32,4,1408]{2,1,0:T(4,128)(2,1)S(1)}, u32[]{:S(2)}, u32[]{:S(2)}) %all-to-all-start) | async-done | bytes 360480 | tf_op jit(solution)/shard_map/all_to_all | solution.py:31
  207.5 0.1 reshape.67
  207.6 1.2 convolution_convert_fusion.1
  208.8 0.7 broadcast_in_dim.20
  209.5 29.4 %all-to-all-start.1 = ((bf16[8,128,128]{2,1,0:T(8,128)(2,1)}), bf16[8,128,128]{2,1,0:T(8,128)(2,1)S(1)}, u32[]{:S(2)}, u32[]{:S(2)}) async-start(bf16[8,128,128]{2,1,0:T(8,128)(2,1)} %broadcast_in_dim.20), calls=%async_computation.2 | async-start | bytes 524288 | tf_op jit(solution)/shard_map/all_to_all | solution.py:31
  238.9 6.5 %all-to-all-done.1 = bf16[8,128,128]{2,1,0:T(8,128)(2,1)S(1)} async-done(((bf16[8,128,128]{2,1,0:T(8,128)(2,1)}), bf16[8,128,128]{2,1,0:T(8,128)(2,1)S(1)}, u32[]{:S(2)}, u32[]{:S(2)}) %all-to-all-start.1) | async-done | bytes 262176 | tf_op jit(solution)/shard_map/all_to_all | solution.py:31
  245.4 0.1 fusion.14
  245.5 0.3 fusion.1
  245.8 0.2 fusion
  246.0 0.1 reshape_reshape.14
  246.1 1.0 reshape_reshape.15
  247.1 0.1 reshape.68
  247.2 1.2 select_maximum_fusion
  248.4 1.4 reshape.69
  249.8 0.1 reduce-scatter.5.cloned.1.call-update
  249.9 93.2 %reduce-scatter.5.cloned.1.call-done = f32[96,128]{1,0:T(8,128)} async-done(((f32[3072,128]{1,0:T(8,128)}), f32[96,128]{1,0:T(8,128)}) %reduce-scatter.5.cloned.1.call-update) | async-done | bytes 49168 | tf_op jit(solution)/shard_map/reduce_scatter | solution.py:21
  343.0 0.8 fusion.29
  343.9 0.7 fusion.24
  344.6 0.1 fusion.21
  344.7 0.1 broadcast_in_dim.21
  344.8 51.8 %all_to_all.26 = bf16[32,4,1408]{2,1,0:T(4,128)(2,1)S(1)} all-to-all(bf16[32,4,1408]{2,1,0:T(4,128)(2,1)S(1)} %broadcast_in_dim.21), channel_id=1, replica_groups=mesh['grp'=2,'ra'=32,'cb'=8] {'ra'}, dimensions={0} | all-to-all | bytes 720896 | tf_op jit(solution)/shard_map/all_to_all | solution.py:31
  396.6 0.1 reshape.73
  396.7 0.3 convolution_convert_fusion
  397.0 35.6 %all_to_all.27 = bf16[8,128,128]{2,1,0:T(8,128)(2,1)S(1)} all-to-all(bf16[8,128,128]{2,1,0:T(8,128)(2,1)S(1)} %broadcast_in_dim.22), channel_id=1, replica_groups=mesh['grp'=2,'ra'=32,'cb'=8] {'cb'}, dimensions={0} | all-to-all | bytes 524288 | tf_op jit(solution)/shard_map/all_to_all | solution.py:31
  432.6 0.1 fusion.4
  432.8 24.4 %all_to_all.28 = f32[32,1,128]{2,1,0:T(1,128)S(1)} all-to-all(f32[32,1,128]{2,1,0:T(1,128)S(1)} %broadcast_in_dim.23), channel_id=1, replica_groups=mesh['grp'=2,'ra'=32,'cb'=8] {'ra'}, dimensions={0} | all-to-all | bytes 32768 | tf_op jit(solution)/shard_map/all_to_all | solution.py:31
  457.1 0.7 fusion.6
  (28 shorter events, 0.3 us)
Async XLA Ops:
  6.5 2.2 copy-start.3
  6.5 147.3 %reduce-scatter.3.cloned.1.call-start = ((), (), s32[]{:S(2)}) async-start(), calls=%async_computation.7 | async-start | bytes 1622016 | tf_op jit(solution)/shard_map/reduce_scatter | solution.py:21
  8.8 1.4 copy-start
  14.4 0.7 copy-start.4
  14.4 0.7 copy-start.5
  14.4 157.8 %copy-start.1 = (f32[2,1408,128]{2,1,0:T(8,128)S(1)}, f32[2,1408,128]{2,1,0:T(8,128)}, u32[]{:S(2)}) copy-start(f32[2,1408,128]{2,1,0:T(8,128)} %param.12) | copy-start | bytes 4325380
  156.3 51.2 %all-to-all-start = ((bf16[32,4,1408]{2,1,0:T(4,128)(2,1)}), bf16[32,4,1408]{2,1,0:T(4,128)(2,1)S(1)}, u32[]{:S(2)}, u32[]{:S(2)}) async-start(bf16[32,4,1408]{2,1,0:T(4,128)(2,1)} %broadcast_in_dim.19), calls=%async_computation.1 | async-start | bytes 720896 | tf_op jit(solution)/shard_map/all_to_all | solution.py:31
  173.2 65.7 %copy-start.6 = (f32[2,128]{1,0:T(2,128)S(1)}, f32[2,128]{1,0:T(2,128)}, u32[]{:S(2)}) copy-start(f32[2,128]{1,0:T(2,128)} %param.15) | copy-start | bytes 3076
  209.5 35.8 %all-to-all-start.1 = ((bf16[8,128,128]{2,1,0:T(8,128)(2,1)}), bf16[8,128,128]{2,1,0:T(8,128)(2,1)S(1)}, u32[]{:S(2)}, u32[]{:S(2)}) async-start(bf16[8,128,128]{2,1,0:T(8,128)(2,1)} %broadcast_in_dim.20), calls=%async_computation.2 | async-start | bytes 524288 | tf_op jit(solution)/shard_map/all_to_all | solution.py:31
  238.9 104.1 %reduce-scatter.5.cloned.1.call-start = ((), (), s32[]{:S(2)}) async-start(), calls=%async_computation.8 | async-start | bytes 1622016 | tf_op jit(solution)/shard_map/reduce_scatter | solution.py:21
  249.8 146.9 %copy-start.2 = (bf16[2,1408,128]{2,1,0:T(8,128)(2,1)S(1)}, bf16[2,1408,128]{2,1,0:T(8,128)(2,1)}, u32[]{:S(2)}) copy-start(bf16[2,1408,128]{2,1,0:T(8,128)(2,1)} %convert.14) | copy-start | bytes 2162692
  396.6 60.5 %copy-start.7 = (f32[128]{0:T(128)S(1)}, f32[128]{0:T(128)}, u32[]{:S(2)}) copy-start(f32[128]{0:T(128)} %param.17) | copy-start | bytes 1540
Sparse Core Ops, SparseCore 0:
  14.5 139.2 reduce-scatter.2
  250.0 92.9 reduce-scatter.4
where the time goes:
time: 466 us; the launch traced here: 465 us
  waiting for transfers between devices  273 us (59%)
  blocking collectives  112 us (24%)
  starting transfers between devices  45.2 us (10%)
  between operations  13.6 us (3%)
  local copies, waits for them, and re-layouts  11.1 us (2%)
  other arithmetic  7.82 us (2%)
    reduce_scatter x2, waiting for transfers between devices, one_scatter(): lax.psum_scatter(lines, axis, tiled=True).reshape(-1)  232 us
    all_to_all x3, blocking collectives, sent_to_all(): return lax.all_to_all(copies, axis, split_axis=0, concat_axis=0, tiled=True)  112 us
    all_to_all x2, starting transfers between devices, sent_to_all(): return lax.all_to_all(copies, axis, split_axis=0, concat_axis=0, tiled=True)  45.2 us
    all_to_all x2, waiting for transfers between devices, sent_to_all(): return lax.all_to_all(copies, axis, split_axis=0, concat_axis=0, tiled=True)  40.8 us
  transfers between devices with their start and end apart: 4, of which 4 were waited for; matrix products, arithmetic and copies ran while one was open for 0% of the time, Pallas kernels for 0%

commit v1 on v0

v1 whole, which is shorter than its diff:
```python
import functools

import jax
import jax.numpy as jnp
from jax import lax
from jax.experimental import pallas as pl
from jax.experimental.pallas import tpu as pltpu
from jax.sharding import PartitionSpec as P

MESH = pl.DeviceIdType.MESH
F32, BF16 = jnp.float32, jnp.bfloat16
LANES, ROWS = 128, 16

PARENT = {9: 0, -9: 0, 3: 0, -3: 0, 6: 9, 12: 9, 15: 9, -6: -9, -12: -9, -14: -9, -15: -14}
for _c in (0, 3, -3, 6, 9, 12, 15, -6, -9, -12):
    PARENT[_c - 1] = _c
    PARENT[_c + 1] = _c
CHILDREN = {}
for _o, _q in PARENT.items():
    CHILDREN.setdefault(_q, []).append(_o)


def height(o):
    return 0 if o not in CHILDREN else 1 + max(height(c) for c in CHILDREN[o])


def path_length(o):
    return 0 if o == 0 else abs(o - PARENT[o]) + path_length(PARENT[o])


def depth(o):
    return 0 if o == 0 else 1 + depth(PARENT[o])


OFFSETS = sorted(PARENT, key=lambda o: (-depth(o), -path_length(o), o))
EDGE = {o: k for k, o in enumerate(OFFSETS)}
INNER = sorted((o for o in CHILDREN if o != 0), key=lambda o: (height(o), -path_length(o), o))
SLOT = {o: k for k, o in enumerate(INNER)}
DOWN = sorted(PARENT, key=lambda o: (depth(o), -height(o), -path_length(o), o))
PEERS = sorted({s * abs(o - q) for o, q in PARENT.items() for s in (1, -1)})
WINDOWS = ((1, "own"), (-1, "own"), (3, "near"), (-3, "near"), (-6, "near"), (5, "pair"), (-9, "right"), (9, "left"))


def body(n_ra, n_cb, layers, width, eps, refs):
    (x_hbm, wg_hbm, wu_hbm, wd_hbm, gs_hbm, us_hbm, ds_hbm, pg_hbm, og_hbm, o_ref,
     x_in, wg, wu, wd, gs, us, ds, pg, og, wgb, wub, wdb, x_ref, pbuf, rbuf, sbuf, hall, cbuf, ssb, ssr, rcol,
     in_sem, rs_s, rs_r, ag_s, ag_r, cb_s, cb_r, ss_s, ss_r) = refs
    z, me = lax.axis_index("ra"), lax.axis_index("cb")
    ff = wg.shape[2]
    cols = ff // LANES
    tok = x_ref.shape[0]
    ttiles = tok // ROWS
    tiles = cols * ttiles
    take = rbuf.shape[1]

    def at(d):
        return lax.rem(z + (n_ra + d), n_ra)

    def start_of(owner):
        return owner * tiles // n_ra

    barrier = pltpu.get_barrier_semaphore()
    for d in PEERS:
        pl.semaphore_signal(barrier, inc=1, device_id={"ra": at(d)}, device_id_type=MESH)
    for k in range(1, n_cb):
        pl.semaphore_signal(barrier, inc=1, device_id={"cb": lax.rem(me + k, n_cb)}, device_id_type=MESH)

    loads = {}

    def load(name, src, dst):
        loads[name] = pltpu.make_async_copy(src, dst, in_sem.at[len(loads)])
        loads[name].start()

    load("x", x_hbm, x_in)
    load("pg", pg_hbm, pg)
    for l in range(layers):
        load(("wg", l), wg_hbm.at[l], wg.at[l])
        load(("wu", l), wu_hbm.at[l], wu.at[l])
        load(("wd", l), wd_hbm.at[l], wd.at[l])
        if l == 0:
            load("gs", gs_hbm, gs)
            load("us", us_hbm, us)
            load("ds", ds_hbm, ds)
            load("og", og_hbm, og)

    def cast(l, which):
        for name, src, dst in (("wg", wg, wgb), ("wu", wu, wub), ("wd", wd, wdb)):
            if name in which:
                loads[(name, l)].wait()
                dst[l] = src[l].astype(BF16)

    def rs_copy(o, src):
        return pltpu.make_async_remote_copy(
            src_ref=src, dst_ref=rbuf.at[EDGE[o]], send_sem=rs_s.at[EDGE[o]], recv_sem=rs_r.at[EDGE[o]],
            device_id={"ra": at(PARENT[o] - o)}, device_id_type=MESH)

    def ss_copy(k):
        kind = {"own": 0, "near": 1, "pair": 2, "right": 3, "left": 4}[WINDOWS[k][1]]
        return pltpu.make_async_remote_copy(
            src_ref=ssb.at[kind], dst_ref=ssr.at[k], send_sem=ss_s.at[k], recv_sem=ss_r.at[k],
            device_id={"ra": at(WINDOWS[k][0])}, device_id_type=MESH)

    def ss_start(xf):
        own = jnp.sum((xf * xf).T, axis=0, keepdims=True)
        ssb[0] = jnp.broadcast_to(own, ssb.shape[1:])
        for k in (0, 1):
            ss_copy(k).start()

    def ss_near():
        for k in (0, 1):
            ss_copy(k).wait_recv()
        ssb[1] = ssb[0] + ssr[0] + ssr[1]
        ssb[2] = ssb[0] + ssr[0]
        for k in (4, 5, 2, 3):
            ss_copy(k).start()

    def ss_mid():
        for k in (2, 3, 4, 5):
            ss_copy(k).wait_recv()
        nine = ssb[1] + ssr[2] + ssr[3]
        ssb[3] = nine + ssr[4]
        ssb[4] = nine + ssr[5]
        ssb[5] = nine
        for k in (6, 7):
            ss_copy(k).start()

    def ss_end():
        for k in (6, 7):
            ss_copy(k).wait_recv()
        total = ssb[5] + ssr[6] + ssr[7]
        for k in range(len(WINDOWS)):
            ss_copy(k).wait_send()
        rinv = lax.rsqrt(total[0:1] / width + eps)
        return jnp.broadcast_to(rinv, (LANES, tok)).T

    loads["x"].wait()
    x_ref[...] = x_in[...].astype(F32)
    loads["pg"].wait()

    for l in range(layers):
        xf = x_ref[...]
        scaled = (xf * pg[l : l + 1, :]).astype(BF16)
        if l == 0:
            cast(0, ("wg", "wu"))
        for which, w in ((0, wgb), (1, wub)):
            part = jnp.dot(scaled, w[l], preferred_element_type=F32).astype(BF16)
            for j in range(cols):
                pbuf[j * ttiles : (j + 1) * ttiles, which] = part[:, j * LANES : (j + 1) * LANES].reshape(
                    ttiles, ROWS, LANES)
        if l == 0:
            pl.semaphore_wait(barrier, len(PEERS) + n_cb - 1)

        for o in OFFSETS:
            if o not in CHILDREN:
                rs_copy(o, pbuf.at[pl.ds(start_of(at(-o)), take)]).start()
        ss_start(xf)
        if l == 0:
            for name in ("gs", "us", "ds", "og"):
                loads[name].wait()
            cast(0, ("wd",))
            for ll in range(1, layers):
                cast(ll, ("wg", "wu", "wd"))

        def total_of(o):
            acc = pbuf[pl.ds(start_of(at(-o)), take)].astype(F32)
            for c in sorted(CHILDREN[o], key=lambda c: (height(c), c)):
                rs_copy(c, rbuf.at[EDGE[c]]).wait_recv()
                acc = acc + rbuf[EDGE[c]].astype(F32)
            return acc

        level = 0
        for o in INNER:
            if height(o) > level:
                level = height(o)
                if level == 1:
                    ss_near()
                if level == 2:
                    ss_mid()
            sbuf[SLOT[o]] = total_of(o).astype(BF16)
            rs_copy(o, sbuf.at[SLOT[o]]).start()
        rcol[...] = ss_end().reshape(ttiles, ROWS, LANES)
        acc = total_of(0)

        first = start_of(z)
        for k in range(take):
            t = first + k
            i, j = lax.rem(t, ttiles), t // ttiles
            rinv = rcol[i]
            at_j = pl.ds(pl.multiple_of(j * LANES, LANES), LANES)
            gate = acc[k, 0] * rinv * gs[l : l + 1, at_j]
            up = acc[k, 1] * rinv * us[l : l + 1, at_j]
            hall[z, k] = (gate / (1.0 + jnp.exp(-gate)) * up).astype(BF16)

        def ag_copy(o, owner):
            return pltpu.make_async_remote_copy(
                src_ref=hall.at[owner], dst_ref=hall.at[owner], send_sem=ag_s.at[EDGE[o]], recv_sem=ag_r.at[EDGE[o]],
                device_id={"ra": at(o - PARENT[o])}, device_id_type=MESH)

        def pass_on(o):
            for c in DOWN:
                if PARENT[c] == o:
                    ag_copy(c, at(-o)).start()

        pass_on(0)
        for o in OFFSETS:
            rs_copy(o, rbuf.at[EDGE[o]]).wait_send()
        for o in DOWN:
            ag_copy(o, at(-o)).wait_recv()
            if o in CHILDREN:
                pass_on(o)
        place = []
        for t in range(tiles):
            owner = max(p for p in range(n_ra) if start_of(p) <= t)
            place.append((owner, t - start_of(owner)))
        hidden = jnp.concatenate(
            [jnp.concatenate([hall[p, k] for p, k in place[j * ttiles : (j + 1) * ttiles]], axis=0) for j in range(cols)],
            axis=1)
        terms = jnp.dot(hidden, wdb[l], preferred_element_type=F32)
        cbuf[l, me] = terms.astype(BF16)

        def cb_copy(k, slot):
            return pltpu.make_async_remote_copy(
                src_ref=cbuf.at[l, slot], dst_ref=cbuf.at[l, slot], send_sem=cb_s.at[l, k], recv_sem=cb_r.at[l, k],
                device_id={"cb": lax.rem(me + k, n_cb)}, device_id_type=MESH)

        for k in range(1, n_cb):
            cb_copy(k, me).start()
        for o in OFFSETS:
            ag_copy(o, at(-o)).wait_send()
        for k in range(1, n_cb):
            cb_copy(k, lax.rem(me + (n_cb - k), n_cb)).wait_recv()
        branch = cbuf[l, 0].astype(F32)
        for k in range(1, n_cb):
            branch = branch + cbuf[l, k].astype(F32)
        for k in range(1, n_cb):
            cb_copy(k, me).wait_send()
        x_ref[...] = (0.5 * xf + branch * ds[l : l + 1, :]).astype(BF16).astype(F32)

    xf = x_ref[...]
    ss_start(xf)
    ss_near()
    ss_mid()
    o_ref[...] = (xf * ss_end() * og[...]).astype(BF16)


def solution(mesh):
    n_ra, n_cb = mesh.shape["ra"], mesh.shape["cb"]

    def local(stream, w_gate, w_up, w_down, gate_scale, up_scale, down_scale, pre_gain, out_gain):
        layers, d_own, ff = w_gate.shape
        tok = stream.shape[0]
        tiles = (ff // LANES) * (tok // ROWS)
        take = -(-tiles // n_ra)
        edges = len(PARENT)
        dma = pltpu.SemaphoreType.DMA
        scratch = [
            pltpu.VMEM(stream.shape, BF16),
            pltpu.VMEM(w_gate.shape, F32),
            pltpu.VMEM(w_up.shape, F32),
            pltpu.VMEM(w_down.shape, F32),
            pltpu.VMEM(gate_scale.shape, F32),
            pltpu.VMEM(up_scale.shape, F32),
            pltpu.VMEM(down_scale.shape, F32),
            pltpu.VMEM(pre_gain.shape, F32),
            pltpu.VMEM((1, d_own), F32),
            pltpu.VMEM(w_gate.shape, BF16),
            pltpu.VMEM(w_up.shape, BF16),
            pltpu.VMEM(w_down.shape, BF16),
            pltpu.VMEM(stream.shape, F32),
            pltpu.VMEM((tiles, 2, ROWS, LANES), BF16),
            pltpu.VMEM((edges, take, 2, ROWS, LANES), BF16),
            pltpu.VMEM((len(INNER), take, 2, ROWS, LANES), BF16),
            pltpu.VMEM((n_ra, take, ROWS, LANES), BF16),
            pltpu.VMEM((layers, n_cb, tok, d_own), BF16),
            pltpu.VMEM((6, 8, tok), F32),
            pltpu.VMEM((len(WINDOWS), 8, tok), F32),
            pltpu.VMEM((tok // ROWS, ROWS, LANES), F32),
            dma((6 + 3 * layers,)),
            dma((edges,)), dma((edges,)), dma((edges,)), dma((edges,)),
            dma((layers, n_cb)), dma((layers, n_cb)),
            dma((len(WINDOWS),)), dma((len(WINDOWS),)),
        ]
        kernel = functools.partial(body, n_ra, n_cb, layers, n_ra * d_own, 1e-6)
        return pl.pallas_call(
            lambda *refs: kernel(refs),
            out_shape=jax.ShapeDtypeStruct(stream.shape, BF16),
            in_specs=[pl.BlockSpec(memory_space=pl.ANY)] * 9,
            out_specs=pl.BlockSpec(memory_space=pltpu.VMEM),
            scratch_shapes=scratch,
            name="ffn_pair",
            compiler_params=pltpu.CompilerParams(collective_id=0, has_side_effects=True),
        )(stream, w_gate, w_up, w_down, gate_scale, up_scale, down_scale, pre_gain, out_gain.reshape(1, d_own))

    placed = (
        P("grp", "ra"),
        P(None, "ra", "cb"),
        P(None, "ra", "cb"),
        P(None, "cb", "ra"),
        P(None, "cb"),
        P(None, "cb"),
        P(None, "ra"),
        P(None, "ra"),
        P("ra"),
    )
    return jax.shard_map(local, mesh=mesh, in_specs=placed, out_specs=P("grp", "ra"), check_vma=False)
```

time: 466 us -> 179 us (0.38)
  waiting for transfers between devices: 273 us -> 0 us
  Pallas kernels: 0 us -> 174 us
  blocking collectives: 112 us -> 0 us
  starting transfers between devices: 45.2 us -> 0 us
  between operations: 13.6 us -> 0.01 us
  local copies, waits for them, and re-layouts: 11.1 us -> 1.38 us
  other arithmetic: 7.82 us -> 0 us
    reduce_scatter x2 -> x0, waiting for transfers between devices: 232 us -> none  [one_scatter(): lax.psum_scatter(lines, axis, tiled=True).reshape(-1)]
    pallas_call x0 -> x1, Pallas kernels: none -> 174 us  [local(): pl.pallas_call(lambda *refs: kernel(refs), out_shape=jax.ShapeDtypeStruct...]
    all_to_all x3 -> x0, blocking collectives: 112 us -> none  [sent_to_all(): return lax.all_to_all(copies, axis, split_axis=0, concat_axis=0, tiled=True)]
    all_to_all x2 -> x0, starting transfers between devices: 45.2 us -> none  [sent_to_all(): return lax.all_to_all(copies, axis, split_axis=0, concat_axis=0, tiled=True)]
    all_to_all x2 -> x0, waiting for transfers between devices: 40.8 us -> none  [sent_to_all(): return lax.all_to_all(copies, axis, split_axis=0, concat_axis=0, tiled=True)]
  transfers between devices with their start and end apart: 4 -> 0, of which waited for: 4 -> 0; matrix products, arithmetic and copies ran while one was open for 0% -> 0% of each run, Pallas kernels for 0% -> 0%
where the time goes in v1:
time: 179 us; the launch traced here: 176 us
  Pallas kernels  174 us (97%)
    pallas_call x1, Pallas kernels, local(): pl.pallas_call(lambda *refs: kernel(refs), out_shape=jax.ShapeDtypeStruct...  174 us

profile of v1, /device:TPU:33, one launch (start us, length us, event | category | flops | bytes accessed | tf_op | source)
XLA Modules:
  0.0 175.7 jit_solution(16606822749637386159)
XLA Ops:
  0.0 174.3 %ffn_pair.1 = bf16[128,128]{1,0:T(8,128)(2,1)} custom-call(bf16[128,128]{1,0:T(8,128)(2,1)} %refs_0_.1, f32[2,128,1408]{2,1,0:T(8,128)} %refs_1_.1, f32[2,128,1408]{2,1,0:T(8,128)} %refs_2_.1, f32[2,1408,128]{2,1,0:T(8,128)} %refs_3_.1, f32[2,1408]{1,0:T(2,128)} %refs_4_.1, f32[2,1408]{1,0:T(2,128)} %refs_5_.1, f32[2,128]{1,0:T(2,128)} %refs_6_.1, ...), custom_call_target="tpu_custom_call" | custom-call | tf_op jit(solution)/shard_map/ffn_pair/pallas_call | solution.py:284
  174.3 1.4 copy.11

commit v2 on v1

--- a/solution.py
+++ b/solution.py
@@ -44,7 +44,7 @@
 def body(n_ra, n_cb, layers, width, eps, refs):
     (x_hbm, wg_hbm, wu_hbm, wd_hbm, gs_hbm, us_hbm, ds_hbm, pg_hbm, og_hbm, o_ref,
      x_in, wg, wu, wd, gs, us, ds, pg, og, wgb, wub, wdb, x_ref, pbuf, rbuf, sbuf, hall, cbuf, ssb, ssr, rcol,
-     in_sem, rs_s, rs_r, ag_s, ag_r, cb_s, cb_r, ss_s, ss_r) = refs
+     in_sem, rs_s, rs_r, ag_s, ag_r, cb_s, cb_r, ss_s, ss_r, fin, fin_s, fin_r) = refs
     z, me = lax.axis_index("ra"), lax.axis_index("cb")
     ff = wg.shape[2]
     cols = ff // LANES
@@ -135,25 +135,26 @@
 
     loads["x"].wait()
     x_ref[...] = x_in[...].astype(F32)
-    loads["pg"].wait()
 
     for l in range(layers):
         xf = x_ref[...]
+        if l == 0:
+            pl.semaphore_wait(barrier, len(PEERS) + n_cb - 1)
+        ss_start(xf)
+        if l == 0:
+            loads["pg"].wait()
+            cast(0, ("wg", "wu"))
         scaled = (xf * pg[l : l + 1, :]).astype(BF16)
-        if l == 0:
-            cast(0, ("wg", "wu"))
         for which, w in ((0, wgb), (1, wub)):
             part = jnp.dot(scaled, w[l], preferred_element_type=F32).astype(BF16)
             for j in range(cols):
                 pbuf[j * ttiles : (j + 1) * ttiles, which] = part[:, j * LANES : (j + 1) * LANES].reshape(
                     ttiles, ROWS, LANES)
-        if l == 0:
-            pl.semaphore_wait(barrier, len(PEERS) + n_cb - 1)
 
         for o in OFFSETS:
             if o not in CHILDREN:
                 rs_copy(o, pbuf.at[pl.ds(start_of(at(-o)), take)]).start()
-        ss_start(xf)
+        ss_near()
         if l == 0:
             for name in ("gs", "us", "ds", "og"):
                 loads[name].wait()
@@ -172,8 +173,6 @@
         for o in INNER:
             if height(o) > level:
                 level = height(o)
-                if level == 1:
-                    ss_near()
                 if level == 2:
                     ss_mid()
             sbuf[SLOT[o]] = total_of(o).astype(BF16)
@@ -237,10 +236,24 @@
         x_ref[...] = (0.5 * xf + branch * ds[l : l + 1, :]).astype(BF16).astype(F32)
 
     xf = x_ref[...]
-    ss_start(xf)
-    ss_near()
-    ss_mid()
-    o_ref[...] = (xf * ss_end() * og[...]).astype(BF16)
+    fin[0:1] = jnp.sum((xf * xf).T, axis=0, keepdims=True)
+
+    def fin_copy(d):
+        k = d % n_ra
+        return pltpu.make_async_remote_copy(
+            src_ref=fin.at[pl.ds(0, 1)], dst_ref=fin.at[pl.ds(k, 1)], send_sem=fin_s.at[k], recv_sem=fin_r.at[k],
+            device_id={"ra": at(d)}, device_id_type=MESH)
+
+    far = [s * d for d in range(n_ra // 2, 0, -1) for s in (1, -1) if 2 * d < n_ra or s > 0]
+    for d in far:
+        fin_copy(d).start()
+    scaled = xf * og[...]
+    for d in far:
+        fin_copy(d).wait_recv()
+    rinv = lax.rsqrt(jnp.sum(fin[...], axis=0, keepdims=True) / width + eps)
+    o_ref[...] = (scaled * jnp.broadcast_to(rinv, (LANES, tok)).T).astype(BF16)
+    for d in far:
+        fin_copy(d).wait_send()
 
 
 def solution(mesh):
@@ -279,6 +292,7 @@
             dma((edges,)), dma((edges,)), dma((edges,)), dma((edges,)),
             dma((layers, n_cb)), dma((layers, n_cb)),
             dma((len(WINDOWS),)), dma((len(WINDOWS),)),
+            pltpu.VMEM((n_ra, tok), F32), dma((n_ra,)), dma((n_ra,)),
         ]
         kernel = functools.partial(body, n_ra, n_cb, layers, n_ra * d_own, 1e-6)
         return pl.pallas_call(

time: 179 us -> 168 us (0.939); the launches traced: 176 us -> 168 us
  Pallas kernels: 174 us -> 166 us
    pallas_call x1, Pallas kernels: 174 us -> 166 us  [local(): pl.pallas_call(lambda *refs: kernel(refs), out_shape=jax.ShapeDtypeStruct...]
where the time goes in v2:
time: 168 us
  Pallas kernels  166 us (99%)
    pallas_call x1, Pallas kernels, local(): pl.pallas_call(lambda *refs: kernel(refs), out_shape=jax.ShapeDtypeStruct...  166 us

profile of v2, /device:TPU:33, one launch (start us, length us, event | category | flops | bytes accessed | tf_op | source)
XLA Modules:
  0.0 167.7 jit_solution(3040289096880454139)
XLA Ops:
  0.0 166.3 %ffn_pair.1 = bf16[128,128]{1,0:T(8,128)(2,1)} custom-call(bf16[128,128]{1,0:T(8,128)(2,1)} %refs_0_.1, f32[2,128,1408]{2,1,0:T(8,128)} %refs_1_.1, f32[2,128,1408]{2,1,0:T(8,128)} %refs_2_.1, f32[2,1408,128]{2,1,0:T(8,128)} %refs_3_.1, f32[2,1408]{1,0:T(2,128)} %refs_4_.1, f32[2,1408]{1,0:T(2,128)} %refs_5_.1, f32[2,128]{1,0:T(2,128)} %refs_6_.1, ...), custom_call_target="tpu_custom_call" | custom-call | tf_op jit(solution)/shard_map/ffn_pair/pallas_call | solution.py:298
  166.3 1.4 copy.11

commit v3 on v2

--- a/solution.py
+++ b/solution.py
@@ -11,34 +11,28 @@
 F32, BF16 = jnp.float32, jnp.bfloat16
 LANES, ROWS = 128, 16
 
-PARENT = {9: 0, -9: 0, 3: 0, -3: 0, 6: 9, 12: 9, 15: 9, -6: -9, -12: -9, -14: -9, -15: -14}
-for _c in (0, 3, -3, 6, 9, 12, 15, -6, -9, -12):
-    PARENT[_c - 1] = _c
-    PARENT[_c + 1] = _c
-CHILDREN = {}
-for _o, _q in PARENT.items():
-    CHILDREN.setdefault(_q, []).append(_o)
+UP = {14: 15, 16: 15, -15: -14, -13: -12, -11: -12, -7: -6, -5: -6, 5: 6, 7: 6, 11: 12, 13: 12, -10: -9, -8: -9, 8:
+    9, 10: 9, -4: -3, -2: -3, 2: 3, 4: 3, -1: 0, 1: 0, 15: 9, -14: -9, -12: -9, -6: -9, 6: 9, 12: 9, -3: 0, 3: 0,
+    -9: 0, 9: 0}
+DOWN = {-9: 0, 9: 0, -3: 0, 3: 0, -1: 0, 1: 0, 15: 9, -14: -9, -12: -9, -6: -9, 6: 9, 12: 9, -10: -9, -8: -9, 8: 9,
+    10: 9, -4: -3, -2: -3, 2: 3, 4: 3, 14: 15, 16: 15, -15: -14, -13: -12, -11: -12, -7: -6, -5: -6, 5: 6, 7: 6,
+    11: 12, 13: 12}
+SUMMED = {}
+for _o, _q in UP.items():
+    SUMMED.setdefault(_q, []).append(_o)
+EDGE = {o: k for k, o in enumerate(c for q in SUMMED for c in SUMMED[q])}
+NODE = {q: k for k, q in enumerate(SUMMED)}
+LEAVES = [o for o in UP if o not in SUMMED]
+INNER = [o for o in UP if o in SUMMED]
 
 
 def height(o):
-    return 0 if o not in CHILDREN else 1 + max(height(c) for c in CHILDREN[o])
-
-
-def path_length(o):
-    return 0 if o == 0 else abs(o - PARENT[o]) + path_length(PARENT[o])
-
-
-def depth(o):
-    return 0 if o == 0 else 1 + depth(PARENT[o])
-
-
-OFFSETS = sorted(PARENT, key=lambda o: (-depth(o), -path_length(o), o))
-EDGE = {o: k for k, o in enumerate(OFFSETS)}
-INNER = sorted((o for o in CHILDREN if o != 0), key=lambda o: (height(o), -path_length(o), o))
-SLOT = {o: k for k, o in enumerate(INNER)}
-DOWN = sorted(PARENT, key=lambda o: (depth(o), -height(o), -path_length(o), o))
-PEERS = sorted({s * abs(o - q) for o, q in PARENT.items() for s in (1, -1)})
+    return 0 if o not in SUMMED else 1 + max(height(c) for c in SUMMED[o])
+
+
 WINDOWS = ((1, "own"), (-1, "own"), (3, "near"), (-3, "near"), (-6, "near"), (5, "pair"), (-9, "right"), (9, "left"))
+REACH = {abs(o - q) for tree in (UP, DOWN) for o, q in tree.items()} | {abs(d) for d, _ in WINDOWS}
+PEERS = sorted(s * d for d in REACH for s in (1, -1))
 
 
 def body(n_ra, n_cb, layers, width, eps, refs):
@@ -83,6 +77,9 @@
             load("ds", ds_hbm, ds)
             load("og", og_hbm, og)
 
+    def wait_for(ref, sem):
+        pltpu.make_async_copy(ref, ref, sem).wait()
+
     def cast(l, which):
         for name, src, dst in (("wg", wg, wgb), ("wu", wu, wub), ("wd", wd, wdb)):
             if name in which:
@@ -91,18 +88,20 @@
 
     def rs_copy(o, src):
         return pltpu.make_async_remote_copy(
-            src_ref=src, dst_ref=rbuf.at[EDGE[o]], send_sem=rs_s.at[EDGE[o]], recv_sem=rs_r.at[EDGE[o]],
-            device_id={"ra": at(PARENT[o] - o)}, device_id_type=MESH)
+            src_ref=src, dst_ref=rbuf.at[EDGE[o]], send_sem=rs_s, recv_sem=rs_r.at[NODE[UP[o]]],
+            device_id={"ra": at(UP[o] - o)}, device_id_type=MESH)
 
     def ss_copy(k):
         kind = {"own": 0, "near": 1, "pair": 2, "right": 3, "left": 4}[WINDOWS[k][1]]
         return pltpu.make_async_remote_copy(
-            src_ref=ssb.at[kind], dst_ref=ssr.at[k], send_sem=ss_s.at[k], recv_sem=ss_r.at[k],
+            src_ref=ssb.at[kind], dst_ref=ssr.at[k], send_sem=ss_s, recv_sem=ss_r.at[k],
             device_id={"ra": at(WINDOWS[k][0])}, device_id_type=MESH)
 
-    def ss_start(xf):
+    def ss_own(xf):
         own = jnp.sum((xf * xf).T, axis=0, keepdims=True)
         ssb[0] = jnp.broadcast_to(own, ssb.shape[1:])
+
+    def ss_start():
         for k in (0, 1):
             ss_copy(k).start()
 
@@ -128,8 +127,6 @@
         for k in (6, 7):
             ss_copy(k).wait_recv()
         total = ssb[5] + ssr[6] + ssr[7]
-        for k in range(len(WINDOWS)):
-            ss_copy(k).wait_send()
         rinv = lax.rsqrt(total[0:1] / width + eps)
         return jnp.broadcast_to(rinv, (LANES, tok)).T
 
@@ -138,9 +135,9 @@
 
     for l in range(layers):
         xf = x_ref[...]
-        if l == 0:
-            pl.semaphore_wait(barrier, len(PEERS) + n_cb - 1)
-        ss_start(xf)
+        ss_own(xf)
+        if l > 0:
+            ss_start()
         if l == 0:
             loads["pg"].wait()
             cast(0, ("wg", "wu"))
@@ -150,33 +147,34 @@
             for j in range(cols):
                 pbuf[j * ttiles : (j + 1) * ttiles, which] = part[:, j * LANES : (j + 1) * LANES].reshape(
                     ttiles, ROWS, LANES)
-
-        for o in OFFSETS:
-            if o not in CHILDREN:
-                rs_copy(o, pbuf.at[pl.ds(start_of(at(-o)), take)]).start()
-        ss_near()
+        if l == 0:
+            pl.semaphore_wait(barrier, len(PEERS) + n_cb - 1)
+            ss_start()
+
+        for o in LEAVES:
+            rs_copy(o, pbuf.at[pl.ds(start_of(at(-o)), take)]).start()
         if l == 0:
             for name in ("gs", "us", "ds", "og"):
                 loads[name].wait()
             cast(0, ("wd",))
             for ll in range(1, layers):
                 cast(ll, ("wg", "wu", "wd"))
+        ss_near()
 
         def total_of(o):
+            wait_for(rbuf.at[pl.ds(EDGE[SUMMED[o][0]], len(SUMMED[o]))], rs_r.at[NODE[o]])
             acc = pbuf[pl.ds(start_of(at(-o)), take)].astype(F32)
-            for c in sorted(CHILDREN[o], key=lambda c: (height(c), c)):
-                rs_copy(c, rbuf.at[EDGE[c]]).wait_recv()
+            for c in SUMMED[o]:
                 acc = acc + rbuf[EDGE[c]].astype(F32)
             return acc
 
-        level = 0
-        for o in INNER:
-            if height(o) > level:
-                level = height(o)
-                if level == 2:
-                    ss_mid()
-            sbuf[SLOT[o]] = total_of(o).astype(BF16)
-            rs_copy(o, sbuf.at[SLOT[o]]).start()
+        nears = sum(height(o) == 1 for o in INNER)
+        slot = {o: k for k, o in enumerate(INNER)}
+        for n, o in enumerate(INNER):
+            if n == nears:
+                ss_mid()
+            sbuf[slot[o]] = total_of(o).astype(BF16)
+            rs_copy(o, sbuf.at[slot[o]]).start()
         rcol[...] = ss_end().reshape(ttiles, ROWS, LANES)
         acc = total_of(0)
 
@@ -190,23 +188,24 @@
             up = acc[k, 1] * rinv * us[l : l + 1, at_j]
             hall[z, k] = (gate / (1.0 + jnp.exp(-gate)) * up).astype(BF16)
 
+        forwards = set(DOWN.values())
+
         def ag_copy(o, owner):
             return pltpu.make_async_remote_copy(
-                src_ref=hall.at[owner], dst_ref=hall.at[owner], send_sem=ag_s.at[EDGE[o]], recv_sem=ag_r.at[EDGE[o]],
-                device_id={"ra": at(o - PARENT[o])}, device_id_type=MESH)
+                src_ref=hall.at[owner], dst_ref=hall.at[owner], send_sem=ag_s, recv_sem=ag_r.at[EDGE[o] if o in forwards else len(EDGE)],
+                device_id={"ra": at(o - DOWN[o])}, device_id_type=MESH)
 
         def pass_on(o):
             for c in DOWN:
-                if PARENT[c] == o:
+                if DOWN[c] == o:
                     ag_copy(c, at(-o)).start()
 
         pass_on(0)
-        for o in OFFSETS:
-            rs_copy(o, rbuf.at[EDGE[o]]).wait_send()
         for o in DOWN:
-            ag_copy(o, at(-o)).wait_recv()
-            if o in CHILDREN:
+            if o in forwards:
+                ag_copy(o, at(-o)).wait_recv()
                 pass_on(o)
+        wait_for(hall.at[pl.ds(0, sum(o not in forwards for o in DOWN))], ag_r.at[len(EDGE)])
         place = []
         for t in range(tiles):
             owner = max(p for p in range(n_ra) if start_of(p) <= t)
@@ -219,20 +218,19 @@
 
         def cb_copy(k, slot):
             return pltpu.make_async_remote_copy(
-                src_ref=cbuf.at[l, slot], dst_ref=cbuf.at[l, slot], send_sem=cb_s.at[l, k], recv_sem=cb_r.at[l, k],
+                src_ref=cbuf.at[l, slot], dst_ref=cbuf.at[l, slot], send_sem=cb_s.at[l], recv_sem=cb_r.at[l],
                 device_id={"cb": lax.rem(me + k, n_cb)}, device_id_type=MESH)
 
         for k in range(1, n_cb):
             cb_copy(k, me).start()
-        for o in OFFSETS:
-            ag_copy(o, at(-o)).wait_send()
-        for k in range(1, n_cb):
-            cb_copy(k, lax.rem(me + (n_cb - k), n_cb)).wait_recv()
+        wait_for(rbuf, rs_s)
+        wait_for(ssr, ss_s)
+        wait_for(hall.at[pl.ds(0, len(DOWN))], ag_s)
+        wait_for(cbuf.at[l, pl.ds(0, n_cb - 1)], cb_r.at[l])
         branch = cbuf[l, 0].astype(F32)
         for k in range(1, n_cb):
             branch = branch + cbuf[l, k].astype(F32)
-        for k in range(1, n_cb):
-            cb_copy(k, me).wait_send()
+        wait_for(cbuf.at[l, pl.ds(0, n_cb - 1)], cb_s.at[l])
         x_ref[...] = (0.5 * xf + branch * ds[l : l + 1, :]).astype(BF16).astype(F32)
 
     xf = x_ref[...]
@@ -241,19 +239,17 @@
     def fin_copy(d):
         k = d % n_ra
         return pltpu.make_async_remote_copy(
-            src_ref=fin.at[pl.ds(0, 1)], dst_ref=fin.at[pl.ds(k, 1)], send_sem=fin_s.at[k], recv_sem=fin_r.at[k],
+            src_ref=fin.at[pl.ds(0, 1)], dst_ref=fin.at[pl.ds(k, 1)], send_sem=fin_s, recv_sem=fin_r,
             device_id={"ra": at(d)}, device_id_type=MESH)
 
     far = [s * d for d in range(n_ra // 2, 0, -1) for s in (1, -1) if 2 * d < n_ra or s > 0]
     for d in far:
         fin_copy(d).start()
     scaled = xf * og[...]
-    for d in far:
-        fin_copy(d).wait_recv()
+    wait_for(fin.at[pl.ds(0, n_ra - 1)], fin_r)
     rinv = lax.rsqrt(jnp.sum(fin[...], axis=0, keepdims=True) / width + eps)
     o_ref[...] = (scaled * jnp.broadcast_to(rinv, (LANES, tok)).T).astype(BF16)
-    for d in far:
-        fin_copy(d).wait_send()
+    wait_for(fin.at[pl.ds(0, n_ra - 1)], fin_s)
 
 
 def solution(mesh):
@@ -264,7 +260,7 @@
         tok = stream.shape[0]
         tiles = (ff // LANES) * (tok // ROWS)
         take = -(-tiles // n_ra)
-        edges = len(PARENT)
+        edges = len(EDGE)
         dma = pltpu.SemaphoreType.DMA
         scratch = [
             pltpu.VMEM(stream.shape, BF16),
@@ -289,10 +285,10 @@
             pltpu.VMEM((len(WINDOWS), 8, tok), F32),
             pltpu.VMEM((tok // ROWS, ROWS, LANES), F32),
             dma((6 + 3 * layers,)),
-            dma((edges,)), dma((edges,)), dma((edges,)), dma((edges,)),
-            dma((layers, n_cb)), dma((layers, n_cb)),
-            dma((len(WINDOWS),)), dma((len(WINDOWS),)),
-            pltpu.VMEM((n_ra, tok), F32), dma((n_ra,)), dma((n_ra,)),
+            dma, dma((len(NODE),)), dma, dma((edges + 1,)),
+            dma((layers,)), dma((layers,)),
+            dma, dma((len(WINDOWS),)),
+            pltpu.VMEM((n_ra, tok), F32), dma, dma,
         ]
         kernel = functools.partial(body, n_ra, n_cb, layers, n_ra * d_own, 1e-6)
         return pl.pallas_call(

time: 168 us -> 166 us (0.988)
  no operation moved by 1% of the time
where the time goes in v3:
time: 166 us
  Pallas kernels  165 us (99%)
    pallas_call x1, Pallas kernels, local(): pl.pallas_call(lambda *refs: kernel(refs), out_shape=jax.ShapeDtypeStruct...  165 us

profile of v3, /device:TPU:33, one launch (start us, length us, event | category | flops | bytes accessed | tf_op | source)
XLA Modules:
  0.0 166.2 jit_solution(13390123047521983948)
XLA Ops:
  0.0 164.9 %ffn_pair.1 = bf16[128,128]{1,0:T(8,128)(2,1)} custom-call(bf16[128,128]{1,0:T(8,128)(2,1)} %refs_0_.1, f32[2,128,1408]{2,1,0:T(8,128)} %refs_1_.1, f32[2,128,1408]{2,1,0:T(8,128)} %refs_2_.1, f32[2,1408,128]{2,1,0:T(8,128)} %refs_3_.1, f32[2,1408]{1,0:T(2,128)} %refs_4_.1, f32[2,1408]{1,0:T(2,128)} %refs_5_.1, f32[2,128]{1,0:T(2,128)} %refs_6_.1, ...), custom_call_target="tpu_custom_call" | custom-call | tf_op jit(solution)/shard_map/ffn_pair/pallas_call | solution.py:294
  164.9 1.4 copy.11

commit v4 on v3

--- a/solution.py
+++ b/solution.py
@@ -11,25 +11,18 @@
 F32, BF16 = jnp.float32, jnp.bfloat16
 LANES, ROWS = 128, 16
 
-UP = {14: 15, 16: 15, -15: -14, -13: -12, -11: -12, -7: -6, -5: -6, 5: 6, 7: 6, 11: 12, 13: 12, -10: -9, -8: -9, 8:
-    9, 10: 9, -4: -3, -2: -3, 2: 3, 4: 3, -1: 0, 1: 0, 15: 9, -14: -9, -12: -9, -6: -9, 6: 9, 12: 9, -3: 0, 3: 0,
-    -9: 0, 9: 0}
-DOWN = {-9: 0, 9: 0, -3: 0, 3: 0, -1: 0, 1: 0, 15: 9, -14: -9, -12: -9, -6: -9, 6: 9, 12: 9, -10: -9, -8: -9, 8: 9,
-    10: 9, -4: -3, -2: -3, 2: 3, 4: 3, 14: 15, 16: 15, -15: -14, -13: -12, -11: -12, -7: -6, -5: -6, 5: 6, 7: 6,
-    11: 12, 13: 12}
+UP = {15: 16, -7: -6, -13: -14, -4: -5, 12: 13, -12: -9, 5: 4, -15: -14, 2: 1, 11: 10, 14: 13, 7: 8, -11: -10,
+    16: 13, 3: 4, 1: 0, -8: -9, -6: -5, 6: 4, -14: -9, -1: -2, 13: 9, -10: -9, 8: 9, -5: -3, 10: 9, 4: 0, -9: 0,
+    -2: -3, 9: 0, -3: 0}
+DOWN = {9: 0, -4: 0, -9: 0, 7: 0, -11: -4, -7: -4, -2: -4, 2: 0, -3: -4, 3: 0, 6: 7, 1: 0, 8: 7, 12: 9, -12: -9, 10: 9,
+    16: 9, -15: -9, -6: -7, 4: 6, 5: 6, -10: -9, -8: -7, -1: 0, 13: 9, 15: 12, 14: 12, 11: 10, -5: -4, -13: -12,
+    -14: -12}
 SUMMED = {}
 for _o, _q in UP.items():
     SUMMED.setdefault(_q, []).append(_o)
 EDGE = {o: k for k, o in enumerate(c for q in SUMMED for c in SUMMED[q])}
 NODE = {q: k for k, q in enumerate(SUMMED)}
-LEAVES = [o for o in UP if o not in SUMMED]
 INNER = [o for o in UP if o in SUMMED]
-
-
-def height(o):
-    return 0 if o not in SUMMED else 1 + max(height(c) for c in SUMMED[o])
-
-
 WINDOWS = ((1, "own"), (-1, "own"), (3, "near"), (-3, "near"), (-6, "near"), (5, "pair"), (-9, "right"), (9, "left"))
 REACH = {abs(o - q) for tree in (UP, DOWN) for o, q in tree.items()} | {abs(d) for d, _ in WINDOWS}
 PEERS = sorted(s * d for d in REACH for s in (1, -1))
@@ -67,15 +60,19 @@
 
     load("x", x_hbm, x_in)
     load("pg", pg_hbm, pg)
-    for l in range(layers):
-        load(("wg", l), wg_hbm.at[l], wg.at[l])
-        load(("wu", l), wu_hbm.at[l], wu.at[l])
-        load(("wd", l), wd_hbm.at[l], wd.at[l])
-        if l == 0:
-            load("gs", gs_hbm, gs)
-            load("us", us_hbm, us)
-            load("ds", ds_hbm, ds)
-            load("og", og_hbm, og)
+    load(("wg", 0), wg_hbm.at[0], wg.at[0])
+    load(("wu", 0), wu_hbm.at[0], wu.at[0])
+
+    def load_rest():
+        load("gs", gs_hbm, gs)
+        load("us", us_hbm, us)
+        load("ds", ds_hbm, ds)
+        load("og", og_hbm, og)
+        load(("wd", 0), wd_hbm.at[0], wd.at[0])
+        for l in range(1, layers):
+            load(("wg", l), wg_hbm.at[l], wg.at[l])
+            load(("wu", l), wu_hbm.at[l], wu.at[l])
+            load(("wd", l), wd_hbm.at[l], wd.at[l])
 
     def wait_for(ref, sem):
         pltpu.make_async_copy(ref, ref, sem).wait()
@@ -151,16 +148,6 @@
             pl.semaphore_wait(barrier, len(PEERS) + n_cb - 1)
             ss_start()
 
-        for o in LEAVES:
-            rs_copy(o, pbuf.at[pl.ds(start_of(at(-o)), take)]).start()
-        if l == 0:
-            for name in ("gs", "us", "ds", "og"):
-                loads[name].wait()
-            cast(0, ("wd",))
-            for ll in range(1, layers):
-                cast(ll, ("wg", "wu", "wd"))
-        ss_near()
-
         def total_of(o):
             wait_for(rbuf.at[pl.ds(EDGE[SUMMED[o][0]], len(SUMMED[o]))], rs_r.at[NODE[o]])
             acc = pbuf[pl.ds(start_of(at(-o)), take)].astype(F32)
@@ -168,13 +155,23 @@
                 acc = acc + rbuf[EDGE[c]].astype(F32)
             return acc
 
-        nears = sum(height(o) == 1 for o in INNER)
-        slot = {o: k for k, o in enumerate(INNER)}
-        for n, o in enumerate(INNER):
-            if n == nears:
+        for o in UP:
+            if o not in SUMMED:
+                rs_copy(o, pbuf.at[pl.ds(start_of(at(-o)), take)]).start()
+                continue
+            n = INNER.index(o)
+            if n == 0:
+                if l == 0:
+                    load_rest()
+                ss_near()
+            if n == len(INNER) // 2:
                 ss_mid()
-            sbuf[slot[o]] = total_of(o).astype(BF16)
-            rs_copy(o, sbuf.at[slot[o]]).start()
+            sbuf[n] = total_of(o).astype(BF16)
+            rs_copy(o, sbuf.at[n]).start()
+        if l == 0:
+            for name in ("gs", "us", "ds", "og"):
+                loads[name].wait()
+            cast(0, ("wd",))
         rcol[...] = ss_end().reshape(ttiles, ROWS, LANES)
         acc = total_of(0)
 
@@ -195,16 +192,15 @@
                 src_ref=hall.at[owner], dst_ref=hall.at[owner], send_sem=ag_s, recv_sem=ag_r.at[EDGE[o] if o in forwards else len(EDGE)],
                 device_id={"ra": at(o - DOWN[o])}, device_id_type=MESH)
 
-        def pass_on(o):
-            for c in DOWN:
-                if DOWN[c] == o:
-                    ag_copy(c, at(-o)).start()
-
-        pass_on(0)
-        for o in DOWN:
-            if o in forwards:
+        held = {0}
+        for c, o in DOWN.items():
+            if o not in held:
+                if l == 0 and len(held) == 1:
+                    for ll in range(1, layers):
+                        cast(ll, ("wg", "wu", "wd"))
                 ag_copy(o, at(-o)).wait_recv()
-                pass_on(o)
+                held.add(o)
+            ag_copy(c, at(-o)).start()
         wait_for(hall.at[pl.ds(0, sum(o not in forwards for o in DOWN))], ag_r.at[len(EDGE)])
         place = []
         for t in range(tiles):

time: 166 us -> 160 us (0.964)
  Pallas kernels: 165 us -> 159 us
    pallas_call x1, Pallas kernels: 165 us -> 159 us  [local(): pl.pallas_call(lambda *refs: kernel(refs), out_shape=jax.ShapeDtypeStruct...]
where the time goes in v4:
time: 160 us
  Pallas kernels  159 us (99%)
    pallas_call x1, Pallas kernels, local(): pl.pallas_call(lambda *refs: kernel(refs), out_shape=jax.ShapeDtypeStruct...  159 us

profile of v4, /device:TPU:33, one launch (start us, length us, event | category | flops | bytes accessed | tf_op | source)
XLA Modules:
  0.0 160.0 jit_solution(16907451543577221924)
XLA Ops:
  0.0 158.7 %ffn_pair.1 = bf16[128,128]{1,0:T(8,128)(2,1)} custom-call(bf16[128,128]{1,0:T(8,128)(2,1)} %refs_0_.1, f32[2,128,1408]{2,1,0:T(8,128)} %refs_1_.1, f32[2,128,1408]{2,1,0:T(8,128)} %refs_2_.1, f32[2,1408,128]{2,1,0:T(8,128)} %refs_3_.1, f32[2,1408]{1,0:T(2,128)} %refs_4_.1, f32[2,1408]{1,0:T(2,128)} %refs_5_.1, f32[2,128]{1,0:T(2,128)} %refs_6_.1, ...), custom_call_target="tpu_custom_call" | custom-call | tf_op jit(solution)/shard_map/ffn_pair/pallas_call | solution.py:290
  158.7 1.4 copy.11

commit v5 on v4

--- a/solution.py
+++ b/solution.py
@@ -11,9 +11,9 @@
 F32, BF16 = jnp.float32, jnp.bfloat16
 LANES, ROWS = 128, 16
 
-UP = {15: 16, -7: -6, -13: -14, -4: -5, 12: 13, -12: -9, 5: 4, -15: -14, 2: 1, 11: 10, 14: 13, 7: 8, -11: -10,
-    16: 13, 3: 4, 1: 0, -8: -9, -6: -5, 6: 4, -14: -9, -1: -2, 13: 9, -10: -9, 8: 9, -5: -3, 10: 9, 4: 0, -9: 0,
-    -2: -3, 9: 0, -3: 0}
+UP = {-11: -9, -14: -13, 10: 11, -7: -8, 2: 1, 16: 13, 12: 13, -15: -12, 14: 13, 15: 13, -13: -12, -8: -9, -1: 0,
+    -4: -5, 6: 7, 5: 4, -6: -5, -10: -9, 11: 9, 13: 8, -12: -9, 7: 8, 9: 8, 3: 1, -3: -2, -5: -2, 4: 1, -9: 0, 8: 0,
+    1: 0, -2: 0}
 DOWN = {9: 0, -4: 0, -9: 0, 7: 0, -11: -4, -7: -4, -2: -4, 2: 0, -3: -4, 3: 0, 6: 7, 1: 0, 8: 7, 12: 9, -12: -9, 10: 9,
     16: 9, -15: -9, -6: -7, 4: 6, 5: 6, -10: -9, -8: -7, -1: 0, 13: 9, 15: 12, 14: 12, 11: 10, -5: -4, -13: -12,
     -14: -12}
@@ -217,7 +217,7 @@
                 src_ref=cbuf.at[l, slot], dst_ref=cbuf.at[l, slot], send_sem=cb_s.at[l], recv_sem=cb_r.at[l],
                 device_id={"cb": lax.rem(me + k, n_cb)}, device_id_type=MESH)
 
-        for k in range(1, n_cb):
+        for k in sorted(range(1, n_cb), key=lambda k: -min(k, n_cb - k)):
             cb_copy(k, me).start()
         wait_for(rbuf, rs_s)
         wait_for(ssr, ss_s)

time: 160 us -> 157 us (0.981)
  Pallas kernels: 159 us -> 156 us
    pallas_call x1, Pallas kernels: 159 us -> 156 us  [local(): pl.pallas_call(lambda *refs: kernel(refs), out_shape=jax.ShapeDtypeStruct...]
where the time goes in v5:
time: 157 us
  Pallas kernels  156 us (99%)
    pallas_call x1, Pallas kernels, local(): pl.pallas_call(lambda *refs: kernel(refs), out_shape=jax.ShapeDtypeStruct...  156 us

profile of v5, /device:TPU:33, one launch (start us, length us, event | category | flops | bytes accessed | tf_op | source)
XLA Modules:
  0.0 157.2 jit_solution(3727912446143232409)
XLA Ops:
  0.0 155.8 %ffn_pair.1 = bf16[128,128]{1,0:T(8,128)(2,1)} custom-call(bf16[128,128]{1,0:T(8,128)(2,1)} %refs_0_.1, f32[2,128,1408]{2,1,0:T(8,128)} %refs_1_.1, f32[2,128,1408]{2,1,0:T(8,128)} %refs_2_.1, f32[2,1408,128]{2,1,0:T(8,128)} %refs_3_.1, f32[2,1408]{1,0:T(2,128)} %refs_4_.1, f32[2,1408]{1,0:T(2,128)} %refs_5_.1, f32[2,128]{1,0:T(2,128)} %refs_6_.1, ...), custom_call_target="tpu_custom_call" | custom-call | tf_op jit(solution)/shard_map/ffn_pair/pallas_call | solution.py:290
  155.8 1.4 copy.11
